TPU v7x, 32 devices: a whole 2x2x4 slice. The times are simulated.
32 devices in a mesh: dp: 4 (over y, x), kv: 4 (over z), tp: 2 (over core).
Axes of the slice: x: 2, y: 2, z: 4, core: 2. Of those that a mesh axis runs over, the one named last changes fastest.
Arguments:
- resid: bfloat16 [16, 2048], P('dp', ('kv', 'tp')), may hold values from -45 to 45
- norm_gain: bfloat16 [3, 2048], P(None, ('kv', 'tp')), may hold values from 0.099609375 to 1.8984375
- ffn_gate: bfloat16 [2, 2048, 5632], P(None, None, ('kv', 'tp')), may hold values from -0.125 to 0.125
- ffn_up: bfloat16 [2, 2048, 5632], P(None, None, ('kv', 'tp')), may hold values from -0.125 to 0.125
- ffn_down: bfloat16 [2, 5632, 2048], P(None, ('kv', 'tp')), may hold values from -0.109375 to 0.109375
- w_x: bfloat16 [2048, 64, 64], P(None, 'kv', 'tp'), may hold values from -0.125 to 0.125
- w_z: bfloat16 [2048, 64, 64], P(None, 'kv', 'tp'), may hold values from -0.125 to 0.125
- w_bc: bfloat16 [2048, 2, 8, 128], P('kv'), may hold values from -0.125 to 0.125
- w_dt: bfloat16 [2048, 64], P('kv'), may hold values from -0.125 to 0.125
- dt_bias: float32 [64], replicated, may hold values from -2 to 0.5
- a_log: float32 [64], replicated, may hold values from -1.5 to 1.5
- d_skip: float32 [64], replicated, may hold values from 0.5 to 1.5
- conv_wx: bfloat16 [4, 64, 64], P(None, None, 'tp'), may hold values from -3 to 3
- conv_wbc: bfloat16 [4, 2, 8, 128], replicated, may hold values from -3 to 3
- conv_x: bfloat16 [16, 3, 64, 64], P(('dp', 'kv'), None, None, 'tp'), may hold values from -6 to 6
- conv_bc: bfloat16 [16, 3, 2, 8, 128], P(('dp', 'kv')), may hold values from -6 to 6
- ssm_state: float32 [16, 64, 64, 128], P(('dp', 'kv'), None, 'tp'), may hold values from -3 to 3
- w_out: bfloat16 [64, 64, 2048], P(None, 'tp', 'kv'), may hold values from -0.09375 to 0.09375
Outputs:
- final: bfloat16 [16, 2048], P('dp', ('kv', 'tp'))
All inputs are finite; a program needn't handle non-finite values.
Results may differ from a plain program's by a relative error of at most 0.018.
Values may be sent and summed in bfloat16 or wider, within the bound.
No kernel may reach another device: no remote copies, remote signals or barrier semaphores. Data moves between devices by JAX's collectives and lax.ppermute only.
A program may use at most 64 MiB of HBM per device.

v0:
```python
import jax
import jax.numpy as jnp
from jax import lax
from jax.sharding import PartitionSpec as P

D = 2048
EPS = 1e-06


def normalize(rows, gain):
    values = rows.astype(jnp.float32)
    scale = lax.rsqrt(jnp.mean(values * values, axis=1, keepdims=True) + EPS)
    return (values * scale * gain.astype(jnp.float32).reshape(1, -1)).astype(jnp.bfloat16)


def feed_forward(normed, w_gate, w_up, w_down):
    gate = jnp.dot(normed, w_gate, preferred_element_type=jnp.float32)
    upper = jnp.dot(normed, w_up, preferred_element_type=jnp.float32)
    hidden = (jax.nn.silu(gate) * upper).astype(jnp.bfloat16)
    return jnp.dot(hidden, w_down, preferred_element_type=jnp.float32)


def add_half(base, sums):
    return (base.astype(jnp.float32) + 0.5 * sums).astype(jnp.bfloat16)


def ffn_totals(partial_value):
    return lax.psum(partial_value, ("kv", "tp"))


def short_conv(history, newest, taps):
    window = jnp.concatenate(
        [history.astype(jnp.float32), newest.astype(jnp.float32)[:, None]], axis=1
    )
    return jax.nn.silu(jnp.sum(window * taps.astype(jnp.float32)[None], axis=1))


def state_step(
    xs_new,
    zeta,
    bc_new,
    dt_raw,
    conv_x,
    conv_bc,
    ssm_state,
    conv_wx,
    conv_wbc,
    dt_bias,
    a_log,
    d_skip,
):
    xconv = short_conv(conv_x, xs_new, conv_wx)
    bconv = short_conv(conv_bc, bc_new, conv_wbc)
    heads = xconv.shape[1]
    groups = bconv.shape[2]
    bmat = jnp.repeat(bconv[:, 0], heads // groups, axis=1)
    cmat = jnp.repeat(bconv[:, 1], heads // groups, axis=1)
    step_size = jax.nn.softplus(dt_raw + dt_bias[None, :])
    decay = jnp.exp(-step_size * jnp.exp(a_log)[None, :])
    updated = (
        decay[:, :, None, None] * ssm_state
        + (step_size[:, :, None] * xconv)[..., None] * bmat[:, :, None, :]
    )
    mixed = (
        jnp.einsum("shpn,shn->shp", updated, cmat, precision=lax.Precision.HIGHEST)
        + d_skip[None, :, None] * xconv
    )
    return (mixed * jax.nn.silu(zeta.astype(jnp.float32))).astype(jnp.bfloat16)


def group_terms(slab, w_bc, w_dt):
    span = slab.shape[1]
    flat_bc = w_bc.reshape(span, -1)
    bc_part = jnp.dot(slab, flat_bc, preferred_element_type=jnp.float32)
    dt_part = jnp.dot(slab, w_dt, preferred_element_type=jnp.float32)
    return (
        lax.psum_scatter(bc_part, "kv", scatter_dimension=0, tiled=True),
        lax.psum_scatter(dt_part, "kv", scatter_dimension=0, tiled=True),
    )


def mix_partial(
    normed,
    w_x,
    w_z,
    w_bc,
    w_dt,
    dt_bias,
    a_log,
    d_skip,
    conv_wx,
    conv_wbc,
    conv_x,
    conv_bc,
    ssm_state,
    w_out,
):
    rows = normed.shape[0]
    local_heads = w_x.shape[1]
    half = w_x.shape[2]
    xs_part = (
        jnp.dot(normed, w_x.reshape(D, -1), preferred_element_type=jnp.float32)
        .astype(jnp.bfloat16)
        .reshape(rows, local_heads, half)
    )
    zeta_part = (
        jnp.dot(normed, w_z.reshape(D, -1), preferred_element_type=jnp.float32)
        .astype(jnp.bfloat16)
        .reshape(rows, local_heads, half)
    )
    xs_new, zeta = (
        lax.all_to_all(xs_part, "kv", split_axis=0, concat_axis=1, tiled=True),
        lax.all_to_all(zeta_part, "kv", split_axis=0, concat_axis=1, tiled=True),
    )
    span = w_bc.shape[0]
    slab = lax.dynamic_slice_in_dim(normed, lax.axis_index("kv") * span, span, 1)
    bc_sum, dt_raw = group_terms(slab, w_bc, w_dt)
    bc_new = bc_sum.astype(jnp.bfloat16).reshape((bc_sum.shape[0],) + w_bc.shape[1:])
    mixed = state_step(
        xs_new,
        zeta,
        bc_new,
        dt_raw,
        conv_x,
        conv_bc,
        ssm_state,
        conv_wx,
        conv_wbc,
        dt_bias,
        a_log,
        d_skip,
    )
    flat_out = w_out.reshape(-1, w_out.shape[2])
    piece = lax.all_gather(mixed, "kv", axis=0, tiled=True)
    return jnp.dot(piece.reshape(piece.shape[0], -1), flat_out, preferred_element_type=jnp.float32)


def per_device(
    resid,
    norm_gain,
    ffn_gate,
    ffn_up,
    ffn_down,
    w_x,
    w_z,
    w_bc,
    w_dt,
    dt_bias,
    a_log,
    d_skip,
    conv_wx,
    conv_wbc,
    conv_x,
    conv_bc,
    ssm_state,
    w_out,
):
    mixer_args = (
        w_x,
        w_z,
        w_bc,
        w_dt,
        dt_bias,
        a_log,
        d_skip,
        conv_wx,
        conv_wbc,
        conv_x,
        conv_bc,
        ssm_state,
        w_out,
    )
    rows, gains = (
        lax.all_gather(resid, ("kv", "tp"), axis=1, tiled=True),
        lax.all_gather(norm_gain, ("kv", "tp"), axis=1, tiled=True),
    )
    first = add_half(
        rows,
        ffn_totals(feed_forward(normalize(rows, gains[0]), ffn_gate[0], ffn_up[0], ffn_down[0])),
    )
    partial_value = mix_partial(normalize(first, gains[1]), *mixer_args)
    span = partial_value.shape[1]
    block = lax.dynamic_slice_in_dim(first, lax.axis_index("kv") * span, span, 1)
    joined = (block.astype(jnp.float32) + lax.psum(partial_value, "tp")).astype(jnp.bfloat16)
    second = lax.all_gather(joined, "kv", axis=1, tiled=True)
    final = add_half(
        second,
        ffn_totals(feed_forward(normalize(second, gains[2]), ffn_gate[1], ffn_up[1], ffn_down[1])),
    )
    width = resid.shape[1]
    return lax.dynamic_slice_in_dim(final, lax.axis_index(("kv", "tp")) * width, width, 1)


def solution(mesh):
    placed = (
        P("dp", ("kv", "tp")),
        P(None, ("kv", "tp")),
        P(None, None, ("kv", "tp")),
        P(None, None, ("kv", "tp")),
        P(None, ("kv", "tp"), None),
        P(None, "kv", "tp"),
        P(None, "kv", "tp"),
        P("kv", None, None, None),
        P("kv", None),
        P(),
        P(),
        P(),
        P(None, None, "tp"),
        P(),
        P(("dp", "kv"), None, None, "tp"),
        P(("dp", "kv"), None, None, None, None),
        P(("dp", "kv"), None, "tp", None),
        P(None, "tp", "kv"),
    )
    return jax.shard_map(
        per_device, mesh=mesh, in_specs=placed, out_specs=P("dp", ("kv", "tp")), check_vma=False
    )
```

profile of v0, /device:TPU:0, one launch (start us, length us, event | category | flops | bytes accessed | tf_op | source)
XLA Modules:
  0.0 168.5 jit_solution(16530086735748407296)
XLA Ops:
  0.0 14.7 %all_gather.12 = bf16[4,2048]{1,0:T(4,128)(2,1)S(1)} all-gather(bf16[4,256]{1,0:T(4,128)(2,1)} %param.18), channel_id=1, replica_groups=mesh['dp'=4,'kv'=4,'tp'=2] {'kv','tp'}, dimensions={1}, use_global_device_ids=true | all-gather | bytes 18432 | tf_op jit(solution)/shard_map/all_gather | solution.py:174
  14.7 0.1 fusion.48
  14.9 12.9 %all_gather.13 = bf16[3,2048]{1,0:T(4,128)(2,1)S(1)} all-gather(bf16[3,256]{1,0:T(4,128)(2,1)} %param.19), channel_id=1, replica_groups=mesh['dp'=4,'kv'=4,'tp'=2] {'kv','tp'}, dimensions={1}, use_global_device_ids=true | all-gather | bytes 13824 | tf_op jit(solution)/shard_map/all_gather | solution.py:175
  27.8 2.7 %fusion.10 = f32[4,704]{1,0:T(4,128)S(1)} fusion(bf16[2,2048,704]{1,2,0:T(8,128)(2,1)} %param.20, bf16[4,2048]{1,0:T(4,128)(2,1)S(1)} %all_gather.12, f32[2048]{0:T(1024)S(1)} %bitcast.113, f32[4]{0:T(128)S(1)} %add_rsqrt_fusion.2), kind=kOutput, calls=%fused_computation.10 | convolution fusion | flops 11567104 | bytes 2919440 | tf_op jit(solution)/shard_map/dot_general | solution.py:17
  30.5 4.4 %fusion.6 = f32[4,2048]{1,0:T(4,128)S(1)} fusion(bf16[2,704,2048]{2,1,0:T(8,128)(2,1)} %param.22, bf16[2,2048,704]{1,2,0:T(8,128)(2,1)} %param.21, f32[4,704]{1,0:T(4,128)S(1)} %fusion.10, bf16[4,2048]{1,0:T(4,128)(2,1)S(1)} %all_gather.12, f32[2048]{0:T(1024)S(1)} %bitcast.114, f32[4]{0:T(128)S(1)} %add_rsqrt_fusion.2), kind=kOutput, calls=%fused_computation.6 | convolution fusion | flops 23118336 | bytes 5835792 | tf_op jit(solution)/shard_map/dot_general | solution.py:20
  34.8 26.7 %psum.21 = f32[4,2048]{1,0:T(4,128)S(1)} all-reduce(f32[4,2048]{1,0:T(4,128)S(1)} %fusion.6), channel_id=1, replica_groups=mesh['dp'=4,'kv'=4,'tp'=2] {'kv','tp'}, use_global_device_ids=true, to_apply=%region_1.2 | all-reduce | flops 8192 | bytes 65536 | tf_op jit(solution)/shard_map/psum | solution.py:28
  61.5 0.1 fusion.45
  61.6 0.1 fusion.47
  61.7 0.0 copy-start.10
  61.7 0.0 copy-start.5
  61.8 0.0 copy-start.6
  61.8 0.0 copy-start.8
  61.8 0.0 copy-start.9
  61.8 0.6 convolution_convert_fusion.1
  62.4 0.0 copy-start.1
  62.5 0.1 reshape.198
  62.5 0.7 reshape.219
  63.2 3.2 %all-to-all-start = ((bf16[4,2,256]{2,1,0:T(2,128)(2,1)}), bf16[4,2,256]{2,1,0:T(2,128)(2,1)S(1)}, u32[]{:S(2)}, u32[]{:S(2)}) async-start(bf16[4,2,256]{2,1,0:T(2,128)(2,1)} %reshape.219), calls=%async_computation | async-start | bytes 8192 | tf_op jit(solution)/shard_map/all_to_all | solution.py:112
  66.5 0.0 copy-start.7
  66.5 2.2 %convolution_convert_fusion = bf16[4,512]{1,0:T(4,128)(2,1)S(1)} fusion(bf16[4,2048]{1,0:T(4,128)(2,1)S(1)} %fusion.47, bf16[2048,512]{0,1:T(8,128)(2,1)} %bitcast.109), kind=kOutput, calls=%fused_computation.26 | convolution fusion | flops 8390656 | bytes 2117632 | tf_op jit(solution)/shard_map/dot_general | solution.py:107
  68.7 0.1 fusion.69
  68.9 2.0 %fusion.18 = f32[4,2048]{1,0:T(4,128)S(1)} fusion(bf16[64,8,16,128]{3,2,1,0:T(8,128)(2,1)} %bitcast.108, bf16[4,2048]{1,0:T(4,128)(2,1)S(1)} %fusion.47, s32[]{:T(128)S(6)} %select_n.11), kind=kOutput, calls=%fused_computation.18 | convolution fusion | flops 8388608 | bytes 2134020 | tf_op jit(solution)/shard_map/dot_general | solution.py:74
  70.9 0.6 dynamic-slice
  71.4 19.8 %all-reduce.2 = (bf16[4,2048]{1,0:T(4,128)(2,1)S(1)}, f32[4,64]{1,0:T(4,128)S(1)}) all-reduce(f32[4,2048]{1,0:T(4,128)S(1)} %fusion.18, f32[4,64]{1,0:T(4,128)S(1)} %fusion.69), channel_id=4, replica_groups=mesh['dp'=4,'kv'=4,'tp'=2] {'kv'}, use_global_device_ids=true, to_apply=%region_5.6.clone | all-reduce | flops 8448 | bytes 51200
  91.2 0.7 fusion.60
  92.0 0.1 reshape.202
  92.1 0.7 reshape.217
  92.7 0.0 all-to-all-done
  92.8 3.2 %all-to-all-start.1 = ((bf16[4,2,256]{2,1,0:T(2,128)(2,1)}), bf16[4,2,256]{2,1,0:T(2,128)(2,1)S(1)}, u32[]{:S(2)}, u32[]{:S(2)}) async-start(bf16[4,2,256]{2,1,0:T(2,128)(2,1)} %reshape.217), calls=%async_computation.1 | async-start | bytes 8192 | tf_op jit(solution)/shard_map/all_to_all | solution.py:113
  96.0 0.7 fusion.75
  96.7 0.1 reshape.220
  96.8 0.1 copy.27
  96.9 4.7 %all-to-all-done.1 = bf16[4,2,256]{2,1,0:T(2,128)(2,1)S(1)} async-done(((bf16[4,2,256]{2,1,0:T(2,128)(2,1)}), bf16[4,2,256]{2,1,0:T(2,128)(2,1)S(1)}, u32[]{:S(2)}, u32[]{:S(2)}) %all-to-all-start.1) | async-done | bytes 4128 | tf_op jit(solution)/shard_map/all_to_all | solution.py:113
  101.6 0.1 reshape.218
  101.7 0.1 copy.30
  101.8 0.1 copy.28
  101.9 1.9 %fusion.33 = f32[64,1,32]{2,1,0:T(1,128)S(1)} fusion(f32[64,128,1]{1,2,0:T(1,128)S(1)} %bitcast.110, f32[1,64,32,128]{3,2,1,0:T(8,128)S(1)} %copy-done.1, f32[64,128]{1,0:T(8,128)S(1)} %broadcast_bitcast_fusion, f32[64,32]{1,0:T(8,128)S(1)} %copy.28, f32[64]{0:T(128)S(1)} %get-tuple-element.7), kind=kOutput, calls=%fused_computation.28 | convolution fusion | flops 3932160 | bytes 1130752 | tf_op jit(solution)/shard_map/shpn,shn->shp/dot_general | solution.py:65
  103.8 0.1 copy.34
  103.9 13.1 %all-gather.1 = bf16[4,64,32]{1,2,0:T(8,128)(2,1)S(1)} all-gather(bf16[1,64,32]{1,2,0:T(8,128)(2,1)S(1)} %fusion.64), channel_id=2, replica_groups=mesh['dp'=4,'kv'=4,'tp'=2] {'kv'}, dimensions={0}, use_global_device_ids=true | all-gather | bytes 20480 | tf_op jit(solution)/shard_map/all_gather | solution.py:134
  117.0 0.1 copy.35
  117.1 2.0 %convolution_bitcast_fusion = f32[4,512]{1,0:T(4,128)S(1)} fusion(bf16[4,64,32]{2,0,1:T(4,128)(2,1)S(1)} %copy.35, bf16[64,32,512]{2,1,0:T(8,128)(2,1)} %param.35), kind=kOutput, calls=%fused_computation.25 | convolution fusion | flops 8388608 | bytes 2121728 | tf_op jit(solution)/shard_map/dot_general | solution.py:135
  119.2 2.5 %psum.22 = f32[4,512]{1,0:T(4,128)S(1)} all-reduce(f32[4,512]{1,0:T(4,128)S(1)} %convolution_bitcast_fusion), channel_id=1, replica_groups=mesh['dp'=4,'kv'=4,'tp'=2] {'tp'}, use_global_device_ids=true, to_apply=%region_7.8 | all-reduce | flops 2048 | bytes 16384 | tf_op jit(solution)/shard_map/psum | solution.py:184
  121.6 13.2 %all_gather.15 = bf16[4,2048]{1,0:T(4,128)(2,1)S(1)} all-gather(bf16[4,512]{1,0:T(4,128)(2,1)S(1)} %add_convert_fusion), channel_id=1, replica_groups=mesh['dp'=4,'kv'=4,'tp'=2] {'kv'}, dimensions={1}, use_global_device_ids=true | all-gather | bytes 20480 | tf_op jit(solution)/shard_map/all_gather | solution.py:185
  134.8 0.1 multiply_reduce_fusion.1
  135.0 2.7 %fusion.4 = f32[4,704]{1,0:T(4,128)S(1)} fusion(bf16[2,2048,704]{1,2,0:T(8,128)(2,1)} %param.20, f32[2048]{0:T(1024)S(1)} %bitcast.111, f32[4]{0:T(128)S(1)} %add_rsqrt_fusion, bf16[4,2048]{1,0:T(4,128)(2,1)S(1)} %all_gather.15), kind=kOutput, calls=%fused_computation.4 | convolution fusion | flops 11567104 | bytes 2919440 | tf_op jit(solution)/shard_map/dot_general | solution.py:17
  137.7 4.4 %fusion = f32[4,2048]{1,0:T(4,128)S(1)} fusion(bf16[2,704,2048]{2,1,0:T(8,128)(2,1)} %param.22, bf16[2,2048,704]{1,2,0:T(8,128)(2,1)} %param.21, f32[4,704]{1,0:T(4,128)S(1)} %fusion.4, f32[2048]{0:T(1024)S(1)} %bitcast.112, f32[4]{0:T(128)S(1)} %add_rsqrt_fusion, bf16[4,2048]{1,0:T(4,128)(2,1)S(1)} %all_gather.15), kind=kOutput, calls=%fused_computation | convolution fusion | flops 23118336 | bytes 5835792 | tf_op jit(solution)/shard_map/dot_general | solution.py:20
  142.0 25.9 %psum.23 = f32[4,2048]{1,0:T(4,128)S(1)} all-reduce(f32[4,2048]{1,0:T(4,128)S(1)} %fusion), channel_id=1, replica_groups=mesh['dp'=4,'kv'=4,'tp'=2] {'kv','tp'}, use_global_device_ids=true, to_apply=%region_9.10 | all-reduce | flops 8192 | bytes 65536 | tf_op jit(solution)/shard_map/psum | solution.py:28
  168.0 0.6 fusion.67
  (30 shorter events, 0.2 us)
Async XLA Ops:
  0.0 61.7 %copy-start = (bf16[2048,16,32]{0,2,1:T(8,128)(2,1)S(1)}, bf16[2048,16,32]{0,2,1:T(8,128)(2,1)}, u32[]{:S(2)}) copy-start(bf16[2048,16,32]{0,2,1:T(8,128)(2,1)} %param.23) | copy-start | bytes 6291460
  34.8 33.9 %copy-start.2 = (bf16[512,64]{0,1:T(8,128)(2,1)S(1)}, bf16[512,64]{0,1:T(8,128)(2,1)}, u32[]{:S(2)}) copy-start(bf16[512,64]{0,1:T(8,128)(2,1)} %param.26) | copy-start | bytes 196612
  61.7 9.1 %copy-start.10 = (u32[32]{0:T(128)S(1)}, u32[32]{0:T(128)}, u32[]{:S(2)}) copy-start(u32[32]{0:T(128)} %constant.45) | copy-start | bytes 388
  61.7 30.2 %copy-start.5 = (bf16[4,2,8,128]{3,2,1,0:T(8,128)(2,1)S(1)}, bf16[4,2,8,128]{3,2,1,0:T(8,128)(2,1)}, u32[]{:S(2)}) copy-start(bf16[4,2,8,128]{3,2,1,0:T(8,128)(2,1)} %param.31) | copy-start | bytes 49156
  61.8 30.2 %copy-start.6 = (bf16[1,3,2,8,128]{4,3,2,1,0:T(8,128)(2,1)S(1)}, bf16[1,3,2,8,128]{4,3,2,1,0:T(8,128)(2,1)}, u32[]{:S(2)}) copy-start(bf16[1,3,2,8,128]{4,3,2,1,0:T(8,128)(2,1)} %param.33) | copy-start | bytes 36868
  61.8 34.2 %copy-start.8 = (f32[64]{0:T(128)S(1)}, f32[64]{0:T(128)}, u32[]{:S(2)}) copy-start(f32[64]{0:T(128)} %param.28) | copy-start | bytes 772
  61.8 34.2 %copy-start.9 = (f32[64]{0:T(128)S(1)}, f32[64]{0:T(128)}, u32[]{:S(2)}) copy-start(f32[64]{0:T(128)} %param.27) | copy-start | bytes 772
  62.4 39.3 %copy-start.3 = (bf16[4,64,32]{1,2,0:T(8,128)(2,1)S(1)}, bf16[4,64,32]{1,2,0:T(8,128)(2,1)}, u32[]{:S(2)}) copy-start(bf16[4,64,32]{1,2,0:T(8,128)(2,1)} %param.30) | copy-start | bytes 49156
  62.4 39.3 %copy-start.4 = (bf16[1,3,64,32]{2,3,1,0:T(8,128)(2,1)S(1)}, bf16[1,3,64,32]{2,3,1,0:T(8,128)(2,1)}, u32[]{:S(2)}) copy-start(bf16[1,3,64,32]{2,3,1,0:T(8,128)(2,1)} %param.32) | copy-start | bytes 36868
  62.4 39.4 %copy-start.1 = (f32[1,64,32,128]{3,2,1,0:T(8,128)S(1)}, f32[1,64,32,128]{3,2,1,0:T(8,128)}, u32[]{:S(2)}) copy-start(f32[1,64,32,128]{3,2,1,0:T(8,128)} %param.34) | copy-start | bytes 3145732
  63.2 29.5 %all-to-all-start = ((bf16[4,2,256]{2,1,0:T(2,128)(2,1)}), bf16[4,2,256]{2,1,0:T(2,128)(2,1)S(1)}, u32[]{:S(2)}, u32[]{:S(2)}) async-start(bf16[4,2,256]{2,1,0:T(2,128)(2,1)} %reshape.219), calls=%async_computation | async-start | bytes 8192 | tf_op jit(solution)/shard_map/all_to_all | solution.py:112
  66.5 37.4 %copy-start.7 = (f32[64]{0:T(128)S(1)}, f32[64]{0:T(128)}, u32[]{:S(2)}) copy-start(f32[64]{0:T(128)} %param.29) | copy-start | bytes 772
  92.8 8.8 %all-to-all-start.1 = ((bf16[4,2,256]{2,1,0:T(2,128)(2,1)}), bf16[4,2,256]{2,1,0:T(2,128)(2,1)S(1)}, u32[]{:S(2)}, u32[]{:S(2)}) async-start(bf16[4,2,256]{2,1,0:T(2,128)(2,1)} %reshape.217), calls=%async_computation.1 | async-start | bytes 8192 | tf_op jit(solution)/shard_map/all_to_all | solution.py:113
where the time goes:
time: 169 us
  blocking collectives  129 us (76%)
  matrix products  22.9 us (14%)
  starting transfers between devices  6.47 us (4%)
  waiting for transfers between devices  4.68 us (3%)
  local copies, waits for them, and re-layouts  3.47 us (2%)
  other arithmetic  1.89 us (1%)
    psum x2, blocking collectives, ffn_totals(): return lax.psum(partial_value, ('kv', 'tp'))  52.6 us
    unnamed x1, blocking collectives  19.8 us
    all_gather x1, blocking collectives, per_device(): lax.all_gather(resid, ('kv', 'tp'), axis=1, tiled=True)  14.7 us
    all_gather x1, blocking collectives, per_device(): second = lax.all_gather(joined, 'kv', axis=1, tiled=True)  13.2 us
    all_gather x1, blocking collectives, mix_partial(): piece = lax.all_gather(mixed, 'kv', axis=0, tiled=True)  13.1 us
    all_gather x1, blocking collectives, per_device(): lax.all_gather(norm_gain, ('kv', 'tp'), axis=1, tiled=True)  12.9 us
    dot_general x2, matrix products, feed_forward(): return jnp.dot(hidden, w_down, preferred_element_type=jnp.float32)  8.72 us
    dot_general x2, matrix products, feed_forward(): gate = jnp.dot(normed, w_gate, preferred_element_type=jnp.float32)  5.31 us
  transfers between devices with their start and end apart: 2, of which 1 were waited for; matrix products, arithmetic and copies ran while one was open for 4% of the time, Pallas kernels for 0%

commit v1 on v0

--- a/solution.py
+++ b/solution.py
@@ -182,7 +182,12 @@
     span = partial_value.shape[1]
     block = lax.dynamic_slice_in_dim(first, lax.axis_index("kv") * span, span, 1)
     joined = (block.astype(jnp.float32) + lax.psum(partial_value, "tp")).astype(jnp.bfloat16)
-    second = lax.all_gather(joined, "kv", axis=1, tiled=True)
+    ring = [joined]
+    for hop in range(3):
+        ring.append(lax.ppermute(ring[-1], "kv", [(dev, (dev + 1) % 4) for dev in range(4)]))
+    second = jnp.roll(
+        jnp.concatenate(ring[::-1], axis=1), (lax.axis_index("kv") + 1) * ring[0].shape[1], axis=1
+    )
     final = add_half(
         second,
         ffn_totals(feed_forward(normalize(second, gains[2]), ffn_gate[1], ffn_up[1], ffn_down[1])),

time: 169 us -> 172 us (1.018)
  waiting for transfers between devices: 4.68 us -> 20.9 us
  blocking collectives: 129 us -> 116 us
    ppermute x0 -> x3, waiting for transfers between devices: none -> 16.2 us  [per_device(): lax.ppermute(ring[-1], 'kv', [(dev, (dev + 1) % 4) for dev in range(4)])]
    all_gather x1 -> x0, blocking collectives: 13.2 us -> none  [per_device(): second = lax.all_gather(joined, 'kv', axis=1, tiled=True)]
  transfers between devices with their start and end apart: 2 -> 5, of which waited for: 1 -> 4; matrix products, arithmetic and copies ran while one was open for 4% -> 4% of each run, Pallas kernels for 0% -> 0%
where the time goes in v1:
time: 172 us
  blocking collectives  116 us (67%)
  matrix products  22.9 us (13%)
  waiting for transfers between devices  20.9 us (12%)
  starting transfers between devices  6.53 us (4%)
  local copies, waits for them, and re-layouts  3.55 us (2%)
  other arithmetic  1.9 us (1%)
    psum x2, blocking collectives, ffn_totals(): return lax.psum(partial_value, ('kv', 'tp'))  52.6 us
    unnamed x1, blocking collectives  19.8 us
    ppermute x3, waiting for transfers between devices, per_device(): lax.ppermute(ring[-1], 'kv', [(dev, (dev + 1) % 4) for dev in range(4)])  16.2 us
    all_gather x1, blocking collectives, per_device(): lax.all_gather(resid, ('kv', 'tp'), axis=1, tiled=True)  14.7 us
    all_gather x1, blocking collectives, mix_partial(): piece = lax.all_gather(mixed, 'kv', axis=0, tiled=True)  13.1 us
    all_gather x1, blocking collectives, per_device(): lax.all_gather(norm_gain, ('kv', 'tp'), axis=1, tiled=True)  12.9 us
    dot_general x2, matrix products, feed_forward(): return jnp.dot(hidden, w_down, preferred_element_type=jnp.float32)  8.72 us
    dot_general x2, matrix products, feed_forward(): gate = jnp.dot(normed, w_gate, preferred_element_type=jnp.float32)  5.32 us
  transfers between devices with their start and end apart: 5, of which 4 were waited for; matrix products, arithmetic and copies ran while one was open for 4% of the time, Pallas kernels for 0%

profile of v1, /device:TPU:0, one launch (start us, length us, event | category | flops | bytes accessed | tf_op | source)
XLA Modules:
  0.0 171.7 jit_solution(15846927619033325398)
XLA Ops:
  0.0 14.7 %all_gather.9 = bf16[4,2048]{1,0:T(4,128)(2,1)S(1)} all-gather(bf16[4,256]{1,0:T(4,128)(2,1)} %param.18), channel_id=1, replica_groups=mesh['dp'=4,'kv'=4,'tp'=2] {'kv','tp'}, dimensions={1}, use_global_device_ids=true | all-gather | bytes 18432 | tf_op jit(solution)/shard_map/all_gather | solution.py:174
  14.7 0.1 fusion.48
  14.9 12.9 %all_gather.10 = bf16[3,2048]{1,0:T(4,128)(2,1)S(1)} all-gather(bf16[3,256]{1,0:T(4,128)(2,1)} %param.19), channel_id=1, replica_groups=mesh['dp'=4,'kv'=4,'tp'=2] {'kv','tp'}, dimensions={1}, use_global_device_ids=true | all-gather | bytes 13824 | tf_op jit(solution)/shard_map/all_gather | solution.py:175
  27.8 2.7 %fusion.10 = f32[4,704]{1,0:T(4,128)S(1)} fusion(bf16[2,2048,704]{1,2,0:T(8,128)(2,1)} %param.20, bf16[4,2048]{1,0:T(4,128)(2,1)S(1)} %all_gather.9, f32[2048]{0:T(1024)S(1)} %bitcast.113, f32[4]{0:T(128)S(1)} %add_rsqrt_fusion.2), kind=kOutput, calls=%fused_computation.10 | convolution fusion | flops 11567104 | bytes 2919440 | tf_op jit(solution)/shard_map/dot_general | solution.py:17
  30.5 4.4 %fusion.6 = f32[4,2048]{1,0:T(4,128)S(1)} fusion(bf16[2,704,2048]{2,1,0:T(8,128)(2,1)} %param.22, bf16[2,2048,704]{1,2,0:T(8,128)(2,1)} %param.21, f32[4,704]{1,0:T(4,128)S(1)} %fusion.10, bf16[4,2048]{1,0:T(4,128)(2,1)S(1)} %all_gather.9, f32[2048]{0:T(1024)S(1)} %bitcast.114, f32[4]{0:T(128)S(1)} %add_rsqrt_fusion.2), kind=kOutput, calls=%fused_computation.6 | convolution fusion | flops 23118336 | bytes 5835792 | tf_op jit(solution)/shard_map/dot_general | solution.py:20
  34.8 26.7 %psum.21 = f32[4,2048]{1,0:T(4,128)S(1)} all-reduce(f32[4,2048]{1,0:T(4,128)S(1)} %fusion.6), channel_id=1, replica_groups=mesh['dp'=4,'kv'=4,'tp'=2] {'kv','tp'}, use_global_device_ids=true, to_apply=%region_1.2 | all-reduce | flops 8192 | bytes 65536 | tf_op jit(solution)/shard_map/psum | solution.py:28
  61.5 0.1 fusion.45
  61.6 0.1 fusion.47
  61.7 0.0 copy-start.10
  61.8 0.0 copy-start.6
  61.8 0.0 copy-start.8
  61.8 0.6 convolution_convert_fusion.1
  62.4 0.0 copy-start.1
  62.5 0.1 reshape.198
  62.5 0.7 reshape.219
  63.2 3.2 %all-to-all-start = ((bf16[4,2,256]{2,1,0:T(2,128)(2,1)}), bf16[4,2,256]{2,1,0:T(2,128)(2,1)S(1)}, u32[]{:S(2)}, u32[]{:S(2)}) async-start(bf16[4,2,256]{2,1,0:T(2,128)(2,1)} %reshape.219), calls=%async_computation | async-start | bytes 8192 | tf_op jit(solution)/shard_map/all_to_all | solution.py:112
  66.5 0.0 copy-start.7
  66.5 2.2 %convolution_convert_fusion = bf16[4,512]{1,0:T(4,128)(2,1)S(1)} fusion(bf16[4,2048]{1,0:T(4,128)(2,1)S(1)} %fusion.47, bf16[2048,512]{0,1:T(8,128)(2,1)} %bitcast.109), kind=kOutput, calls=%fused_computation.26 | convolution fusion | flops 8390656 | bytes 2117632 | tf_op jit(solution)/shard_map/dot_general | solution.py:107
  68.7 0.1 fusion.69
  68.9 2.0 %fusion.18 = f32[4,2048]{1,0:T(4,128)S(1)} fusion(bf16[64,8,16,128]{3,2,1,0:T(8,128)(2,1)} %bitcast.108, bf16[4,2048]{1,0:T(4,128)(2,1)S(1)} %fusion.47, s32[]{:T(128)S(6)} %select_n.24), kind=kOutput, calls=%fused_computation.18 | convolution fusion | flops 8388608 | bytes 2134020 | tf_op jit(solution)/shard_map/dot_general | solution.py:74
  70.9 0.6 dynamic-slice
  71.4 19.8 %all-reduce.2 = (bf16[4,2048]{1,0:T(4,128)(2,1)S(1)}, f32[4,64]{1,0:T(4,128)S(1)}) all-reduce(f32[4,2048]{1,0:T(4,128)S(1)} %fusion.18, f32[4,64]{1,0:T(4,128)S(1)} %fusion.69), channel_id=4, replica_groups=mesh['dp'=4,'kv'=4,'tp'=2] {'kv'}, use_global_device_ids=true, to_apply=%region_5.6.clone | all-reduce | flops 8448 | bytes 51200
  91.2 0.7 fusion.60
  92.0 0.1 reshape.202
  92.1 0.7 reshape.217
  92.8 3.2 %all-to-all-start.1 = ((bf16[4,2,256]{2,1,0:T(2,128)(2,1)}), bf16[4,2,256]{2,1,0:T(2,128)(2,1)S(1)}, u32[]{:S(2)}, u32[]{:S(2)}) async-start(bf16[4,2,256]{2,1,0:T(2,128)(2,1)} %reshape.217), calls=%async_computation.1 | async-start | bytes 8192 | tf_op jit(solution)/shard_map/all_to_all | solution.py:113
  96.0 0.7 fusion.75
  96.7 0.1 reshape.220
  96.8 0.1 copy.27
  96.9 4.7 %all-to-all-done.1 = bf16[4,2,256]{2,1,0:T(2,128)(2,1)S(1)} async-done(((bf16[4,2,256]{2,1,0:T(2,128)(2,1)}), bf16[4,2,256]{2,1,0:T(2,128)(2,1)S(1)}, u32[]{:S(2)}, u32[]{:S(2)}) %all-to-all-start.1) | async-done | bytes 4128 | tf_op jit(solution)/shard_map/all_to_all | solution.py:113
  101.6 0.1 reshape.218
  101.7 0.1 copy.30
  101.8 0.1 copy.28
  101.9 1.9 %fusion.33 = f32[64,1,32]{2,1,0:T(1,128)S(1)} fusion(f32[64,128,1]{1,2,0:T(1,128)S(1)} %bitcast.110, f32[1,64,32,128]{3,2,1,0:T(8,128)S(1)} %copy-done.1, f32[64,128]{1,0:T(8,128)S(1)} %broadcast_bitcast_fusion, f32[64,32]{1,0:T(8,128)S(1)} %copy.28, f32[64]{0:T(128)S(1)} %get-tuple-element.7), kind=kOutput, calls=%fused_computation.28 | convolution fusion | flops 3932160 | bytes 1130752 | tf_op jit(solution)/shard_map/shpn,shn->shp/dot_general | solution.py:65
  103.8 0.1 copy.34
  103.9 13.1 %all-gather.1 = bf16[4,64,32]{1,2,0:T(8,128)(2,1)S(1)} all-gather(bf16[1,64,32]{1,2,0:T(8,128)(2,1)S(1)} %fusion.64), channel_id=2, replica_groups=mesh['dp'=4,'kv'=4,'tp'=2] {'kv'}, dimensions={0}, use_global_device_ids=true | all-gather | bytes 20480 | tf_op jit(solution)/shard_map/all_gather | solution.py:134
  117.0 0.1 copy.35
  117.1 2.0 %convolution_bitcast_fusion = f32[4,512]{1,0:T(4,128)S(1)} fusion(bf16[4,64,32]{2,0,1:T(4,128)(2,1)S(1)} %copy.35, bf16[64,32,512]{2,1,0:T(8,128)(2,1)} %param.35), kind=kOutput, calls=%fused_computation.25 | convolution fusion | flops 8388608 | bytes 2121728 | tf_op jit(solution)/shard_map/dot_general | solution.py:135
  119.2 2.5 %psum.22 = f32[4,512]{1,0:T(4,128)S(1)} all-reduce(f32[4,512]{1,0:T(4,128)S(1)} %convolution_bitcast_fusion), channel_id=1, replica_groups=mesh['dp'=4,'kv'=4,'tp'=2] {'tp'}, use_global_device_ids=true, to_apply=%region_7.8 | all-reduce | flops 2048 | bytes 16384 | tf_op jit(solution)/shard_map/psum | solution.py:184
  121.6 0.1 collective-permute-start
  121.7 5.4 %collective-permute-done = bf16[4,512]{1,0:T(4,128)(2,1)S(1)} collective-permute-done((bf16[4,512]{1,0:T(4,128)(2,1)S(1)}, bf16[4,512]{1,0:T(4,128)(2,1)S(1)}, u32[]{:S(2)}, u32[]{:S(2)}) %collective-permute-start) | collective-permute-done | bytes 4128 | tf_op jit(solution)/shard_map/ppermute | solution.py:187
  127.1 5.4 %collective-permute-done.1 = bf16[4,512]{1,0:T(4,128)(2,1)S(1)} collective-permute-done((bf16[4,512]{1,0:T(4,128)(2,1)S(1)}, bf16[4,512]{1,0:T(4,128)(2,1)S(1)}, u32[]{:S(2)}, u32[]{:S(2)}) %collective-permute-start.1) | collective-permute-done | bytes 4128 | tf_op jit(solution)/shard_map/ppermute | solution.py:187
  132.5 5.4 %collective-permute-done.2 = bf16[4,512]{1,0:T(4,128)(2,1)S(1)} collective-permute-done((bf16[4,512]{1,0:T(4,128)(2,1)S(1)}, bf16[4,512]{1,0:T(4,128)(2,1)S(1)}, u32[]{:S(2)}, u32[]{:S(2)}) %collective-permute-start.2) | collective-permute-done | bytes 4128 | tf_op jit(solution)/shard_map/ppermute | solution.py:187
  138.0 0.1 multiply_reduce_fusion.1
  138.2 2.7 %fusion.4 = f32[4,704]{1,0:T(4,128)S(1)} fusion(bf16[2,2048,704]{1,2,0:T(8,128)(2,1)} %param.20, f32[2048]{0:T(1024)S(1)} %bitcast.111, f32[4]{0:T(128)S(1)} %add_rsqrt_fusion, bf16[4,4096]{1,0:T(4,128)(2,1)S(1)} %constant_dynamic-update-slice_fusion, s32[]{:T(128)S(6)} %select_n.27), kind=kOutput, calls=%fused_computation.4 | convolution fusion | flops 11567104 | bytes 2919940 | tf_op jit(solution)/shard_map/dot_general | solution.py:17
  140.8 4.4 %fusion = f32[4,2048]{1,0:T(4,128)S(1)} fusion(bf16[2,704,2048]{2,1,0:T(8,128)(2,1)} %param.22, bf16[2,2048,704]{1,2,0:T(8,128)(2,1)} %param.21, f32[4,704]{1,0:T(4,128)S(1)} %fusion.4, f32[2048]{0:T(1024)S(1)} %bitcast.112, f32[4]{0:T(128)S(1)} %add_rsqrt_fusion, bf16[4,4096]{1,0:T(4,128)(2,1)S(1)} %constant_dynamic-update-slice_fusion, s32[]{:T(128)S(6)} %select_n.27), kind=kOutput, calls=%fused_computation | convolution fusion | flops 23118336 | bytes 5837316 | tf_op jit(solution)/shard_map/dot_general | solution.py:20
  145.2 25.9 %psum.23 = f32[4,2048]{1,0:T(4,128)S(1)} all-reduce(f32[4,2048]{1,0:T(4,128)S(1)} %fusion), channel_id=1, replica_groups=mesh['dp'=4,'kv'=4,'tp'=2] {'kv','tp'}, use_global_device_ids=true, to_apply=%region_9.10 | all-reduce | flops 8192 | bytes 65536 | tf_op jit(solution)/shard_map/psum | solution.py:28
  171.1 0.6 fusion.67
  (43 shorter events, 0.3 us)
Async XLA Ops:
  0.0 61.7 %copy-start = (bf16[2048,16,32]{0,2,1:T(8,128)(2,1)S(1)}, bf16[2048,16,32]{0,2,1:T(8,128)(2,1)}, u32[]{:S(2)}) copy-start(bf16[2048,16,32]{0,2,1:T(8,128)(2,1)} %param.23) | copy-start | bytes 6291460
  34.8 33.9 %copy-start.2 = (bf16[512,64]{0,1:T(8,128)(2,1)S(1)}, bf16[512,64]{0,1:T(8,128)(2,1)}, u32[]{:S(2)}) copy-start(bf16[512,64]{0,1:T(8,128)(2,1)} %param.26) | copy-start | bytes 196612
  61.7 9.1 %copy-start.10 = (u32[32]{0:T(128)S(1)}, u32[32]{0:T(128)}, u32[]{:S(2)}) copy-start(u32[32]{0:T(128)} %constant.67) | copy-start | bytes 388
  61.7 30.2 %copy-start.5 = (bf16[4,2,8,128]{3,2,1,0:T(8,128)(2,1)S(1)}, bf16[4,2,8,128]{3,2,1,0:T(8,128)(2,1)}, u32[]{:S(2)}) copy-start(bf16[4,2,8,128]{3,2,1,0:T(8,128)(2,1)} %param.31) | copy-start | bytes 49156
  61.8 30.2 %copy-start.6 = (bf16[1,3,2,8,128]{4,3,2,1,0:T(8,128)(2,1)S(1)}, bf16[1,3,2,8,128]{4,3,2,1,0:T(8,128)(2,1)}, u32[]{:S(2)}) copy-start(bf16[1,3,2,8,128]{4,3,2,1,0:T(8,128)(2,1)} %param.33) | copy-start | bytes 36868
  61.8 34.2 %copy-start.8 = (f32[64]{0:T(128)S(1)}, f32[64]{0:T(128)}, u32[]{:S(2)}) copy-start(f32[64]{0:T(128)} %param.28) | copy-start | bytes 772
  61.8 34.2 %copy-start.9 = (f32[64]{0:T(128)S(1)}, f32[64]{0:T(128)}, u32[]{:S(2)}) copy-start(f32[64]{0:T(128)} %param.27) | copy-start | bytes 772
  62.4 39.3 %copy-start.3 = (bf16[4,64,32]{1,2,0:T(8,128)(2,1)S(1)}, bf16[4,64,32]{1,2,0:T(8,128)(2,1)}, u32[]{:S(2)}) copy-start(bf16[4,64,32]{1,2,0:T(8,128)(2,1)} %param.30) | copy-start | bytes 49156
  62.4 39.3 %copy-start.4 = (bf16[1,3,64,32]{2,3,1,0:T(8,128)(2,1)S(1)}, bf16[1,3,64,32]{2,3,1,0:T(8,128)(2,1)}, u32[]{:S(2)}) copy-start(bf16[1,3,64,32]{2,3,1,0:T(8,128)(2,1)} %param.32) | copy-start | bytes 36868
  62.4 39.4 %copy-start.1 = (f32[1,64,32,128]{3,2,1,0:T(8,128)S(1)}, f32[1,64,32,128]{3,2,1,0:T(8,128)}, u32[]{:S(2)}) copy-start(f32[1,64,32,128]{3,2,1,0:T(8,128)} %param.34) | copy-start | bytes 3145732
  63.2 29.5 %all-to-all-start = ((bf16[4,2,256]{2,1,0:T(2,128)(2,1)}), bf16[4,2,256]{2,1,0:T(2,128)(2,1)S(1)}, u32[]{:S(2)}, u32[]{:S(2)}) async-start(bf16[4,2,256]{2,1,0:T(2,128)(2,1)} %reshape.219), calls=%async_computation | async-start | bytes 8192 | tf_op jit(solution)/shard_map/all_to_all | solution.py:112
  66.5 37.4 %copy-start.7 = (f32[64]{0:T(128)S(1)}, f32[64]{0:T(128)}, u32[]{:S(2)}) copy-start(f32[64]{0:T(128)} %param.29) | copy-start | bytes 772
  92.8 8.8 %all-to-all-start.1 = ((bf16[4,2,256]{2,1,0:T(2,128)(2,1)}), bf16[4,2,256]{2,1,0:T(2,128)(2,1)S(1)}, u32[]{:S(2)}, u32[]{:S(2)}) async-start(bf16[4,2,256]{2,1,0:T(2,128)(2,1)} %reshape.217), calls=%async_computation.1 | async-start | bytes 8192 | tf_op jit(solution)/shard_map/all_to_all | solution.py:113
  121.6 5.5 %collective-permute-start = (bf16[4,512]{1,0:T(4,128)(2,1)S(1)}, bf16[4,512]{1,0:T(4,128)(2,1)S(1)}, u32[]{:S(2)}, u32[]{:S(2)}) collective-permute-start(bf16[4,512]{1,0:T(4,128)(2,1)S(1)} %add_convert_fusion), channel_id=1, source_target_pairs={{0,2},{2,4},{4,6},{6,0},{1,3},{3,5},{5,7},{7,1},{8,10},{10,12},{12... | collective-permute-start | bytes 12296 | tf_op jit(solution)/shard_map/ppermute | solution.py:187
  127.1 5.4 %collective-permute-start.1 = (bf16[4,512]{1,0:T(4,128)(2,1)S(1)}, bf16[4,512]{1,0:T(4,128)(2,1)S(1)}, u32[]{:S(2)}, u32[]{:S(2)}) collective-permute-start(bf16[4,512]{1,0:T(4,128)(2,1)S(1)} %collective-permute-done), channel_id=1, source_target_pairs={{0,2},{2,4},{4,6},{6,0},{1,3},{3,5},{5,7},{7,1},{8,10},{10,12},{12... | collective-permute-start | bytes 12296 | tf_op jit(solution)/shard_map/ppermute | solution.py:187
  132.5 5.4 %collective-permute-start.2 = (bf16[4,512]{1,0:T(4,128)(2,1)S(1)}, bf16[4,512]{1,0:T(4,128)(2,1)S(1)}, u32[]{:S(2)}, u32[]{:S(2)}) collective-permute-start(bf16[4,512]{1,0:T(4,128)(2,1)S(1)} %collective-permute-done.1), channel_id=1, source_target_pairs={{0,2},{2,4},{4,6},{6,0},{1,3},{3,5},{5,7},{7,1},{8,10},{10,12},{12... | collective-permute-start | bytes 12296 | tf_op jit(solution)/shard_map/ppermute | solution.py:187
